TPU v7x, 32 devices: a whole 2x2x4 slice. The times are simulated.
32 devices in a mesh: sp: 8 (over z, y), tp: 4 (over x, core).
Axes of the slice: x: 2, y: 2, z: 4, core: 2. Of those that a mesh axis runs over, the one named last changes fastest.
Arguments:
- queries: bfloat16 [4096, 1024], P('sp', 'tp'), may hold values from -6 to 6
- keys: bfloat16 [4096, 1024], P('sp', 'tp'), may hold values from -6 to 6
- values: bfloat16 [4096, 1024], P('sp', 'tp'), may hold values from -12 to 12
- breaks: bfloat16 [4096, 8], P('sp', 'tp'), may hold values from -12 to 0.5
- residual_in: bfloat16 [4096, 2048], P('sp', 'tp'), may hold values from -6 to 6
- out_weight: bfloat16 [1024, 2048], P('tp'), may hold values from -0.1875 to 0.1875
- first_gain: float32 [2048], replicated, may hold values from 0.1 to 1.9
- first_shift: float32 [2048], replicated, may hold values from -2 to 2
- up_weight: bfloat16 [2048, 8192], P('sp', 'tp'), may hold values from -0.125 to 0.125
- down_weight: bfloat16 [2048, 8192], P('sp', 'tp'), may hold values from -0.0625 to 0.0625
- second_gain: float32 [2048], replicated, may hold values from 0.1 to 1.9
- second_shift: float32 [2048], replicated, may hold values from -2 to 2
Outputs:
- layer_out: bfloat16 [4096, 2048], P('sp', 'tp')
All inputs are finite; a program needn't handle non-finite values.
Results may differ from a plain program's by a relative error of at most 0.018.
Values may be sent and summed in bfloat16 or wider, within the bound.
A program may use at most 128 MiB of HBM per device.

v0:
```python
import jax
import jax.numpy as jnp
from jax import lax
from jax.sharding import PartitionSpec as P

D = 2048
KEY_BLOCK = 512


ALPHA = 2.0**0.25
EPSILON = 1e-05


def collect(up_weight, down_weight):
    return (
        lax.all_gather(up_weight, "sp", axis=0, tiled=True),
        lax.all_gather(down_weight, "sp", axis=0, tiled=True),
    )


def attend_rows(query_rows, first_pos, keys_all, values_all, breaks_all, heads_here):
    tok_rows = query_rows.shape[0]
    head_size = query_rows.shape[1] // heads_here
    scale = head_size ** (-0.5)
    block_count = (first_pos + tok_rows + KEY_BLOCK - 1) // KEY_BLOCK
    query_heads = query_rows.reshape(tok_rows, heads_here, head_size)
    query_pos = first_pos + jnp.arange(tok_rows, dtype=jnp.int32)

    def visit(turn, carry):
        later_sum, totals = carry
        start = (block_count - 1 - turn) * KEY_BLOCK
        key_tile_rows = lax.dynamic_slice_in_dim(keys_all, start, KEY_BLOCK, 0).reshape(
            KEY_BLOCK, heads_here, head_size
        )
        value_block = lax.dynamic_slice_in_dim(values_all, start, KEY_BLOCK, 0).reshape(
            KEY_BLOCK, heads_here, head_size
        )
        break_block = lax.dynamic_slice_in_dim(breaks_all, start, KEY_BLOCK, 0).astype(jnp.float32)
        scores = (
            jnp.einsum(
                "qhd,khd->hqk", query_heads, key_tile_rows, preferred_element_type=jnp.float32
            )
            * scale
        )
        scores = scores + break_block.T[:, None, :]
        key_pos = start + jnp.arange(KEY_BLOCK, dtype=jnp.int32)
        strict = (key_pos[None, :] < query_pos[:, None])[None]
        log_break = jax.nn.log_sigmoid(scores)
        log_keep = jnp.where(strict, log_break - scores, 0.0)
        later = lax.cumsum(log_keep, axis=2, reverse=True) - log_keep + later_sum[:, :, None]
        weights = jnp.where(strict, jnp.exp(log_break + later), 0.0).astype(jnp.bfloat16)
        totals = totals + jnp.einsum(
            "hqk,khd->qhd", weights, value_block, preferred_element_type=jnp.float32
        )
        return (later_sum + jnp.sum(log_keep, axis=2), totals)

    start_state = (
        jnp.zeros((heads_here, tok_rows), jnp.float32),
        jnp.zeros((tok_rows, heads_here, head_size), jnp.float32),
    )
    totals = lax.fori_loop(0, block_count, visit, start_state)[1]
    return totals.reshape(tok_rows, heads_here * head_size).astype(jnp.bfloat16)


def attend(queries, keys, values, breaks):
    keys_all, values_all, breaks_all = (
        lax.all_gather(keys, "sp", axis=0, tiled=True),
        lax.all_gather(values, "sp", axis=0, tiled=True),
        lax.all_gather(breaks, "sp", axis=0, tiled=True),
    )
    tok_rows = queries.shape[0]
    heads_here = breaks.shape[1]
    offset = lax.axis_index("sp") * tok_rows
    return attend_rows(queries, offset, keys_all, values_all, breaks_all, heads_here)


def normalize(pre, gain, shift):
    row_sum, row_squares = lax.psum((jnp.sum(pre, axis=-1), jnp.sum(pre * pre, axis=-1)), "tp")
    center = row_sum / D
    spread = row_squares / D - center * center
    return (pre - center[:, None]) * lax.rsqrt(spread + EPSILON)[:, None] * gain + shift


def body(
    queries,
    keys,
    values,
    breaks,
    residual_in,
    out_weight,
    first_gain,
    first_shift,
    up_weight,
    down_weight,
    second_gain,
    second_shift,
):
    attended = attend(queries, keys, values, breaks)
    up_full, down_full = collect(up_weight, down_weight)
    columns = residual_in.shape[1]
    column_start = lax.axis_index("tp") * columns
    partial_value = jnp.dot(attended, out_weight, preferred_element_type=jnp.float32)
    mixed = lax.psum(partial_value.astype(jnp.bfloat16), "tp").astype(jnp.float32)
    residual_full = lax.all_gather(residual_in, "tp", axis=1, tiled=True)
    pre = ALPHA * residual_full.astype(jnp.float32) + mixed
    center = jnp.mean(pre, axis=-1, keepdims=True)
    centered = pre - center
    spread = jnp.mean(centered * centered, axis=-1, keepdims=True)
    first_full = (centered * lax.rsqrt(spread + EPSILON) * first_gain + first_shift).astype(
        jnp.bfloat16
    )
    hidden_pre = jnp.dot(first_full, up_full, preferred_element_type=jnp.float32)
    first_out = lax.dynamic_slice_in_dim(first_full, column_start, columns, 1)
    activated = jnp.square(jax.nn.relu(hidden_pre)).astype(jnp.bfloat16)
    hidden_partial = lax.dot_general(
        activated, down_full, (((1,), (1,)), ((), ())), preferred_element_type=jnp.float32
    )
    channel_mix = lax.psum_scatter(
        hidden_partial.astype(jnp.bfloat16), "tp", scatter_dimension=1, tiled=True
    ).astype(jnp.float32)
    second_pre = ALPHA * first_out.astype(jnp.float32) + channel_mix
    gain_second = lax.dynamic_slice_in_dim(second_gain, column_start, columns, 0)
    shift_second = lax.dynamic_slice_in_dim(second_shift, column_start, columns, 0)
    return normalize(second_pre, gain_second, shift_second).astype(jnp.bfloat16)


def solution(mesh):
    return jax.shard_map(
        body,
        mesh=mesh,
        in_specs=(
            P("sp", "tp"),
            P("sp", "tp"),
            P("sp", "tp"),
            P("sp", "tp"),
            P("sp", "tp"),
            P("tp", None),
            P(),
            P(),
            P("sp", "tp"),
            P("sp", "tp"),
            P(),
            P(),
        ),
        out_specs=P("sp", "tp"),
        check_vma=False,
    )
```

profile of v0, /device:TPU:27, one launch (start us, length us, event | category | flops | bytes accessed | tf_op | source)
XLA Modules:
  0.0 647.2 jit_solution(15874895582837259042)
XLA Ops:
  12.1 18.5 %all_gather.20 = bf16[4096,2]{0,1:T(2,128)(2,1)S(1)} all-gather(bf16[512,2]{0,1:T(2,128)(2,1)S(1)} %copy-done.11), channel_id=1, replica_groups=mesh['sp'=8,'tp'=4] {'sp'}, dimensions={0}, use_global_device_ids=true | all-gather | bytes 18432 | tf_op jit(solution)/shard_map/all_gather | solution.py:69
  30.6 28.4 %all-gather.10.cloned.1.call-done = bf16[4096,256]{0,1:T(8,128)(2,1)} async-done(((bf16[512,256]{0,1:T(8,128)(2,1)}), bf16[4096,256]{0,1:T(8,128)(2,1)}) %all-gather.10.cloned.1.call-update) | async-done | bytes 2097168 | tf_op jit(solution)/shard_map/all_gather | solution.py:68
  59.0 50.6 %all-gather.8.cloned.1.call-done = bf16[4096,256]{0,1:T(8,128)(2,1)} async-done(((bf16[512,256]{0,1:T(8,128)(2,1)}), bf16[4096,256]{0,1:T(8,128)(2,1)}) %all-gather.8.cloned.1.call-update) | async-done | bytes 2097168 | tf_op jit(solution)/shard_map/all_gather | solution.py:67
  110.4 148.4 %while.15 = (s32[]{:T(128)}, f32[2,512]{1,0:T(2,128)S(1)}, f32[512,2,128]{0,2,1:T(8,128)}, s32[]{:T(128)}, s32[]{:T(128)}, /*index=5*/bf16[4096,256]{0,1:T(8,128...) while((s32[]{:T(128)}, f32[2,512]{1,0:T(2,128)S(1)}, ...), condition=%wide.region_4.5_spmd.clone, body=%wide.region_0.4_spmd.clone.sunk | while | flops 351683584 | bytes 40532296 | solution.py:61
  112.4 4.1 fusion.39
  116.5 9.6 %fusion.40 = f32[2,512,4,128]{1,2,3,0:T(4,128)S(1)} fusion(f32[2,512,4,128]{1,3,2,0:T(8,128)S(1)} %bitcast.75), kind=kOutput, calls=%fused_computation.12.clone.1 | output fusion | flops 66584576 | bytes 4194304 | tf_op jit(solution)/shard_map/reduce-window.4
  128.2 2.3 fusion.41
  133.6 4.1 fusion.39
  137.7 9.6 %fusion.40 = f32[2,512,4,128]{1,2,3,0:T(4,128)S(1)} fusion(f32[2,512,4,128]{1,3,2,0:T(8,128)S(1)} %bitcast.75), kind=kOutput, calls=%fused_computation.12.clone.1 | output fusion | flops 66584576 | bytes 4194304 | tf_op jit(solution)/shard_map/reduce-window.4
  149.4 2.3 fusion.41
  154.9 4.1 fusion.39
  158.9 9.6 %fusion.40 = f32[2,512,4,128]{1,2,3,0:T(4,128)S(1)} fusion(f32[2,512,4,128]{1,3,2,0:T(8,128)S(1)} %bitcast.75), kind=kOutput, calls=%fused_computation.12.clone.1 | output fusion | flops 66584576 | bytes 4194304 | tf_op jit(solution)/shard_map/reduce-window.4
  170.6 2.3 fusion.41
  176.1 4.1 fusion.39
  180.1 9.6 %fusion.40 = f32[2,512,4,128]{1,2,3,0:T(4,128)S(1)} fusion(f32[2,512,4,128]{1,3,2,0:T(8,128)S(1)} %bitcast.75), kind=kOutput, calls=%fused_computation.12.clone.1 | output fusion | flops 66584576 | bytes 4194304 | tf_op jit(solution)/shard_map/reduce-window.4
  191.8 2.3 fusion.41
  197.3 4.1 fusion.39
  201.3 9.6 %fusion.40 = f32[2,512,4,128]{1,2,3,0:T(4,128)S(1)} fusion(f32[2,512,4,128]{1,3,2,0:T(8,128)S(1)} %bitcast.75), kind=kOutput, calls=%fused_computation.12.clone.1 | output fusion | flops 66584576 | bytes 4194304 | tf_op jit(solution)/shard_map/reduce-window.4
  218.5 4.1 fusion.39
  222.6 9.6 %fusion.40 = f32[2,512,4,128]{1,2,3,0:T(4,128)S(1)} fusion(f32[2,512,4,128]{1,3,2,0:T(8,128)S(1)} %bitcast.75), kind=kOutput, calls=%fused_computation.12.clone.1 | output fusion | flops 66584576 | bytes 4194304 | tf_op jit(solution)/shard_map/reduce-window.4
  234.2 2.3 fusion.41
  239.7 4.1 fusion.39
  243.8 9.6 %fusion.40 = f32[2,512,4,128]{1,2,3,0:T(4,128)S(1)} fusion(f32[2,512,4,128]{1,3,2,0:T(8,128)S(1)} %bitcast.75), kind=kOutput, calls=%fused_computation.12.clone.1 | output fusion | flops 66584576 | bytes 4194304 | tf_op jit(solution)/shard_map/reduce-window.4
  255.4 2.3 fusion.41
  263.3 70.5 %all-reduce.3.cloned.1.call-done = bf16[512,2048]{1,0:T(8,128)(2,1)} async-done(((bf16[512,2048]{1,0:T(8,128)(2,1)}), bf16[512,2048]{1,0:T(8,128)(2,1)}) %all-reduce.3.cloned.1.call-update) | async-done | bytes 2097168 | tf_op jit(solution)/shard_map/psum | solution.py:103
  333.8 3.1 fusion.13
  338.0 2.5 add_convert_fusion
  340.6 118.9 %all-gather.12.cloned.1.call-done = bf16[2048,2048]{1,0:T(8,128)(2,1)} async-done(((bf16[256,2048]{1,0:T(8,128)(2,1)}), bf16[2048,2048]{1,0:T(8,128)(2,1)}) %all-gather.12.cloned.1.call-update) | async-done | bytes 8388624 | tf_op jit(solution)/shard_map/all_gather | solution.py:16
  459.5 124.7 %all-gather.14.cloned.1.call-done = bf16[2048,2048]{1,0:T(8,128)(2,1)} async-done(((bf16[256,2048]{1,0:T(8,128)(2,1)}), bf16[2048,2048]{1,0:T(8,128)(2,1)}) %all-gather.14.cloned.1.call-update) | async-done | bytes 8388624 | tf_op jit(solution)/shard_map/all_gather | solution.py:17
  584.1 16.5 %convolution_convert_fusion.1 = bf16[512,2048]{1,0:T(8,128)(2,1)} fusion(bf16[2048,2048]{1,0:T(8,128)(2,1)} %all-gather.14.cloned.1.call-done, bf16[512,2048]{1,0:T(8,128)(2,1)} %add_convert_fusion, bf16[2048,2048]{1,0:T(8,128)(2,1)} %all-gather.12.cloned.1.call-done), kind=kOutput, calls=%fused_computation.32 | convolution fusion | flops 8594128896 | bytes 20971520 | tf_op jit(solution)/shard_map/dot_general | solution.py:115
  602.3 28.6 %reduce-scatter.2.cloned.1.call-done = bf16[512,512]{1,0:T(8,128)(2,1)} async-done(((bf16[512,2048]{1,0:T(8,128)(2,1)}), bf16[512,512]{1,0:T(8,128)(2,1)}) %reduce-scatter.2.cloned.1.call-update) | async-done | bytes 524304 | tf_op jit(solution)/shard_map/reduce_scatter | solution.py:118
  632.3 5.9 all-reduce
  (181 shorter events, 55.0 us)
Async XLA Ops:
  6.5 253.4 %copy-start = (bf16[256,2048]{1,0:T(8,128)(2,1)S(1)}, bf16[256,2048]{1,0:T(8,128)(2,1)}, u32[]{:S(2)}) copy-start(bf16[256,2048]{1,0:T(8,128)(2,1)} %param.19) | copy-start | bytes 3145732
  6.5 4.6 copy-start.8
  6.5 5.6 copy-start.11
  6.5 52.4 %all-gather.10.cloned.1.call-start = ((), (), s32[]{:S(2)}) async-start(), calls=%async_computation.3 | async-start | bytes 2359296 | tf_op jit(solution)/shard_map/all_gather | solution.py:68
  8.5 101.1 %all-gather.8.cloned.1.call-start = ((), (), s32[]{:S(2)}) async-start(), calls=%async_computation.2 | async-start | bytes 2359296 | tf_op jit(solution)/shard_map/all_gather | solution.py:67
  10.3 252.9 %all-gather.6.cloned.1.call-start = ((), (), s32[]{:S(2)}) async-start(), calls=%async_computation.1 | async-start | bytes 2621440 | tf_op jit(solution)/shard_map/all_gather | solution.py:104
  11.1 322.7 %all-reduce.3.cloned.1.call-start = ((), (), s32[]{:S(2)}) async-start(), calls=%async_computation.4 | async-start | bytes 4194304 | tf_op jit(solution)/shard_map/psum | solution.py:103
  126.6 1.6 copy-start.1
  128.2 2.3 copy-start.2
  128.2 2.3 copy-start.3
  147.8 1.6 copy-start.1
  149.4 2.3 copy-start.2
  149.4 2.3 copy-start.3
  169.0 1.6 copy-start.1
  170.6 2.3 copy-start.2
  170.6 2.3 copy-start.3
  190.2 1.6 copy-start.1
  191.8 2.3 copy-start.2
  191.8 2.3 copy-start.3
  213.0 2.3 copy-start.2
  213.0 2.3 copy-start.3
  234.2 2.3 copy-start.2
  234.2 2.3 copy-start.3
  253.8 1.6 copy-start.1
  255.4 2.3 copy-start.2
  255.4 2.3 copy-start.3
  262.1 197.4 %all-gather.12.cloned.1.call-start = ((), (), s32[]{:S(2)}) async-start(), calls=%async_computation.5 | async-start | bytes 9437184 | tf_op jit(solution)/shard_map/all_gather | solution.py:16
  262.7 321.5 %all-gather.14.cloned.1.call-start = ((), (), s32[]{:S(2)}) async-start(), calls=%async_computation.6 | async-start | bytes 9437184 | tf_op jit(solution)/shard_map/all_gather | solution.py:17
  263.2 367.7 %reduce-scatter.2.cloned.1.call-start = ((), (), s32[]{:S(2)}) async-start(), calls=%async_computation.7 | async-start | bytes 2621440 | tf_op jit(solution)/shard_map/reduce_scatter | solution.py:118
  263.3 73.7 %copy-start.5 = (bf16[512,2048]{1,0:T(8,128)(2,1)S(1)}, bf16[512,2048]{1,0:T(8,128)(2,1)}, u32[]{:S(2)}) copy-start(bf16[512,2048]{1,0:T(8,128)(2,1)} %all-gather.6.cloned.1.call-done) | copy-start | bytes 6291460
  333.8 3.1 copy-start.6
  600.6 30.3 %copy-start.7 = (bf16[512,2048]{1,0:T(8,128)(2,1)S(1)}, bf16[512,2048]{1,0:T(8,128)(2,1)}, u32[]{:S(2)}) copy-start(bf16[512,2048]{1,0:T(8,128)(2,1)} %add_convert_fusion) | copy-start | bytes 6291460
  (11 other events, 10.9 us)
Sparse Core Ops, SparseCore 0:
  9.4 49.5 all-gather.9
  61.0 48.5 all-gather.7
  111.2 22.0 all-gather.5
  262.2 71.5 all-reduce.2
  335.8 123.6 all-gather.11
  461.5 122.6 all-gather.13
  600.8 30.0 reduce-scatter.1
where the time goes:
time: 651 us; the launch traced here: 647 us
  waiting for transfers between devices  423 us (65%)
  other arithmetic  99.3 us (15%)
  matrix products  49.4 us (8%)
  local copies, waits for them, and re-layouts  36.1 us (6%)
  blocking collectives  24.3 us (4%)
  between operations  13.6 us (2%)
    all_gather x1, waiting for transfers between devices, collect(): lax.all_gather(down_weight, 'sp', axis=0, tiled=True)  125 us
    all_gather x1, waiting for transfers between devices, collect(): lax.all_gather(up_weight, 'sp', axis=0, tiled=True)  119 us
    psum x1, waiting for transfers between devices, body(): lax.psum(partial_value.astype(jnp.bfloat16), 'tp').astype(jnp.float32)  70.5 us
    another operation x14, other arithmetic  67.7 us
    all_gather x1, waiting for transfers between devices, attend(): lax.all_gather(keys, 'sp', axis=0, tiled=True)  50.6 us
    dot_general x7, matrix products, visit(): jnp.einsum('qhd,khd->hqk', query_heads, key_tile_rows, preferred_element_...  28.6 us
    reduce_scatter x1, waiting for transfers between devices, body(): lax.psum_scatter(hidden_partial.astype(jnp.bfloat16), 'tp', scatter_dimen...  28.6 us
    all_gather x1, waiting for transfers between devices, attend(): lax.all_gather(values, 'sp', axis=0, tiled=True)  28.4 us
  transfers between devices with their start and end apart: 7, of which 6 were waited for; matrix products, arithmetic and copies ran while one was open for 23% of the time, Pallas kernels for 0%

commit v1 on v0

v1 whole, which is shorter than its diff:
```python
import functools

import jax
import jax.numpy as jnp
from jax import lax
from jax.experimental import pallas as pl
from jax.experimental.pallas import tpu as pltpu
from jax.sharding import PartitionSpec as P

ALPHA = 2.0**0.25
EPSILON = 1e-05
MESH = pl.DeviceIdType.MESH
F32 = jnp.float32
BF16 = jnp.bfloat16
KV, UP, DOWN = 0, 1, 2
RIGHT, LEFT = 0, 1


def aligned(start, size):
    return pl.ds(pl.multiple_of(start, size), size)


def layer_kernel(
    n,
    t,
    heads,
    q_ref,
    kv_in,
    br_in,
    res_in,
    ow_in,
    g1_ref,
    b1_ref,
    up_in,
    down_in,
    g2_ref,
    b2_ref,
    out_ref,
    kv,
    up,
    down,
    br,
    ow,
    res,
    later_sum,
    totals,
    att_all,
    lower,
    pre,
    first,
    activated,
    part,
    mix,
    stat,
    ring_send,
    ring_recv,
    br_send,
    br_recv,
    ow_send,
    ow_recv,
    res_send,
    res_recv,
    att_send,
    att_recv,
    mix_send,
    mix_recv,
    stat_send,
    stat_recv,
    local_sem,
):
    me = lax.axis_index("sp")
    me_t = lax.axis_index("tp")
    tok = q_ref.shape[0]
    width = q_ref.shape[1]
    hd = width // heads
    feat = first.shape[1]
    cols = feat // t
    block = feat // n
    per = n // t
    half_n = n // 2

    def at_pos(p):
        p = lax.rem(p + n, n)
        back = p // half_n
        return 2 * (p + back * (n - 1 - 2 * p)) + back

    pos = me // 2 + lax.rem(me, 2) * (n - 1 - 2 * (me // 2))
    next_dev = (at_pos(pos + 1), at_pos(pos - 1))
    own_in = (kv_in, up_in, down_in)
    full = (kv, up, down)
    rows_of = (tok, block, block)

    def ring_copy(item, way, hop, piece, own=False):
        rows = rows_of[item]
        half = rows // 2
        owner = at_pos(pos - (hop - 1) if way == RIGHT else pos + (hop - 1))
        dst = full[item].at[aligned(owner * rows + piece * half, half)]
        src = own_in[item].at[aligned(piece * half, half)] if own else dst
        return pltpu.make_async_remote_copy(
            src_ref=src,
            dst_ref=dst,
            send_sem=ring_send.at[item, way, hop, piece],
            recv_sem=ring_recv.at[item, way, hop, piece],
            device_id={"sp": next_dev[way]},
            device_id_type=MESH,
        )

    def ring_landed(item, way, hop, piece):
        rows = rows_of[item]
        half = rows // 2
        owner = at_pos(pos - hop if way == RIGHT else pos + hop)
        dst = full[item].at[aligned(owner * rows + piece * half, half)]
        return pltpu.make_async_remote_copy(
            src_ref=dst,
            dst_ref=dst,
            send_sem=ring_send.at[item, way, hop, piece],
            recv_sem=ring_recv.at[item, way, hop, piece],
            device_id={"sp": next_dev[way]},
            device_id_type=MESH,
        )

    def start_own(item):
        ring_copy(item, RIGHT, 1, 0, own=True).start()
        ring_copy(item, LEFT, 1, 1, own=True).start()
        ring_copy(item, RIGHT, 1, 1, own=True).start()
        ring_copy(item, LEFT, 1, 0, own=True).start()

    def event(item, e, hop=None, second=None):
        static = isinstance(e, int)
        hop = 1 + e // 2
        second = e % 2 if static else lax.rem(e, 2)
        ring_landed(item, RIGHT, hop, second).wait_recv()

        def forward_right():
            ring_copy(item, RIGHT, hop + 1, second).start()

        def forward_left():
            ring_copy(item, LEFT, hop + 1, 1 - second).start()

        def start_next():
            if item < DOWN:
                start_own(item + 1)

        def guarded(cond, fn):
            if static:
                if cond:
                    fn()
            else:
                pl.when(cond)(fn)

        guarded(e < n - 3, forward_right)
        ring_landed(item, LEFT, hop, 1 - second).wait_recv()
        guarded(e < n - 3, forward_left)
        guarded(e == n - 4, start_next)

    def drain_sends(item):
        def one(e, _):
            hop = 1 + e // 2
            second = lax.rem(e, 2)
            ring_copy(item, RIGHT, hop, second).wait_send()
            ring_copy(item, LEFT, hop, 1 - second).wait_send()
            return 0

        lax.fori_loop(0, n - 1, one, 0)

    def peer_t(d):
        return lax.rem(me_t + d, t)

    def tp_copy(src, dst_of, sends, recvs, d):
        return pltpu.make_async_remote_copy(
            src_ref=src,
            dst_ref=dst_of(me_t),
            send_sem=sends.at[d],
            recv_sem=recvs.at[d],
            device_id={"tp": peer_t(d)},
            device_id_type=MESH,
        )

    def tp_landed(dst_of, sends, recvs, d):
        dst = dst_of(lax.rem(me_t + t - d, t))
        return pltpu.make_async_remote_copy(
            src_ref=dst,
            dst_ref=dst,
            send_sem=sends.at[d],
            recv_sem=recvs.at[d],
            device_id={"tp": peer_t(d)},
            device_id_type=MESH,
        )

    def br_copy(d, landed=False):
        owner = lax.rem(me + n - d, n) if landed else me
        return pltpu.make_async_remote_copy(
            src_ref=br.at[owner] if landed else br_in,
            dst_ref=br.at[owner],
            send_sem=br_send.at[d],
            recv_sem=br_recv.at[d],
            device_id={"sp": lax.rem(me + d, n)},
            device_id_type=MESH,
        )

    barrier = pltpu.get_barrier_semaphore()

    def greet(d, _):
        pl.semaphore_signal(
            barrier, inc=1, device_id={"sp": lax.rem(me + d, n)}, device_id_type=MESH
        )
        return 0

    lax.fori_loop(1, n, greet, 0)
    for d in range(1, t):
        pl.semaphore_signal(barrier, inc=1, device_id={"tp": peer_t(d)}, device_id_type=MESH)

    res_at = lambda g: res.at[g]
    ow_at = lambda g: ow.at[g]
    att_at = lambda g: att_all.at[g]

    locals_ = [
        pltpu.make_async_copy(kv_in, kv.at[aligned(me * tok, tok)], local_sem.at[0]),
        pltpu.make_async_copy(up_in, up.at[aligned(me * block, block)], local_sem.at[1]),
        pltpu.make_async_copy(down_in, down.at[aligned(me * block, block)], local_sem.at[2]),
        pltpu.make_async_copy(br_in, br.at[me], local_sem.at[3]),
        pltpu.make_async_copy(res_in, res.at[me_t], local_sem.at[4]),
        pltpu.make_async_copy(ow_in, ow.at[me_t], local_sem.at[5]),
    ]
    pl.semaphore_wait(barrier, n - 1 + t - 1)
    start_own(KV)

    def send_breaks(d, _):
        br_copy(d).start()
        return 0

    lax.fori_loop(1, n, send_breaks, 0)
    for c in locals_:
        c.start()
    for d in range(1, t):
        tp_copy(ow_in, ow_at, ow_send, ow_recv, d).start()
    for d in range(1, t):
        tp_copy(res_in, res_at, res_send, res_recv, d).start()

    key_row = lax.broadcasted_iota(jnp.int32, (tok, tok), 0)
    key_col = lax.broadcasted_iota(jnp.int32, (tok, tok), 1)
    lower[...] = jnp.where(key_row > key_col, 1.0, 0.0).astype(BF16)
    later_sum[...] = jnp.zeros_like(later_sum)
    totals[...] = jnp.zeros_like(totals)

    def kv_event(e, _):
        event(KV, e)
        return 0

    lax.fori_loop(0, n - 2, kv_event, 0)

    def last_event(item):
        ring_landed(item, RIGHT, half_n, 0).wait_recv()
        ring_landed(item, LEFT, half_n, 1).wait_recv()

    last_event(KV)

    def wait_breaks(d, _):
        br_copy(d, landed=True).wait_recv()
        return 0

    lax.fori_loop(1, n, wait_breaks, 0)
    for c in locals_:
        c.wait()

    scale = hd ** (-0.5)
    tile = 128

    def attend_block(j):
        b = me - j
        for h in range(heads):
            def rows(i, _):
                at = aligned(i * tile, tile)
                keys = kv[aligned(b * tok, tok), pl.ds(h * hd, hd)]
                vals = kv[aligned(b * tok, tok), pl.ds(width + h * hd, hd)]
                z = lax.dot_general(
                    q_ref[at, pl.ds(h * hd, hd)],
                    keys,
                    (((1,), (1,)), ((), ())),
                    preferred_element_type=F32,
                )
                z = z * scale + br[b, pl.ds(h, 1), :]
                soft = jnp.log(1.0 + jnp.exp(-jnp.abs(z)))
                log_break = jnp.minimum(z, 0.0) - soft
                r = lax.broadcasted_iota(jnp.int32, (tile, tok), 0) + i * tile + j * tok
                strict = lax.broadcasted_iota(jnp.int32, (tile, tok), 1) < r
                log_keep = jnp.where(strict, log_break - z, 0.0)
                high = log_keep.astype(BF16)
                low = (log_keep - high.astype(F32)).astype(BF16)
                tri = lower[...]
                later = jnp.dot(high, tri, preferred_element_type=F32) + jnp.dot(
                    low, tri, preferred_element_type=F32
                )
                before = later_sum[h, at, :]
                w = jnp.exp(log_break + later + before[:, 0:1])
                w = jnp.where(strict, w, 0.0).astype(BF16)
                totals[at, pl.ds(h * hd, hd)] += jnp.dot(w, vals, preferred_element_type=F32)
                later_sum[h, at, :] = before + jnp.sum(log_keep, axis=1, keepdims=True)
                return 0

            lax.fori_loop(0, tok // tile, rows, 0)

    def attend_step(j, _):
        @pl.when(j <= me)
        def _():
            attend_block(j)

        @pl.when(j < n - 2)
        def _():
            event(UP, j)

        return 0

    lax.fori_loop(0, n, attend_step, 0)

    own_att = att_all.at[me_t]
    own_att[...] = totals[...].astype(BF16)
    for d in range(1, t):
        tp_copy(own_att, att_at, att_send, att_recv, d).start()
    last_event(UP)
    for d in range(1, t):
        tp_landed(ow_at, ow_send, ow_recv, d).wait_recv()
        tp_landed(res_at, res_send, res_recv, d).wait_recv()
    for d in range(1, t):
        tp_landed(att_at, att_send, att_recv, d).wait_recv()

    big = 256

    def mix_rows(i, _):
        at = aligned(i * big, big)
        for c in range(t):
            lanes = pl.ds(c * cols, cols)
            acc = ALPHA * res[c, at, :].astype(F32)
            mixed = jnp.zeros((big, cols), F32)
            for g in range(t):
                mixed = mixed + jnp.dot(
                    att_all[g, at, :], ow[g, :, lanes], preferred_element_type=F32
                ).astype(BF16).astype(F32)
            pre[at, lanes] = acc + mixed
        return 0

    lax.fori_loop(0, tok // big, mix_rows, 0)
    event(DOWN, 0)

    small = 64

    def norm_rows(i, _):
        at = aligned(i * small, small)
        x = pre[at, :]
        center = jnp.sum(x, axis=1, keepdims=True) / feat
        x = x - center
        spread = jnp.sum(x * x, axis=1, keepdims=True) / feat
        first[at, :] = (x * lax.rsqrt(spread + EPSILON) * g1_ref[...] + b1_ref[...]).astype(BF16)
        return 0

    lax.fori_loop(0, tok // small, norm_rows, 0)

    hidden = up.shape[1]
    strip = 256

    def up_cols(i, _):
        lanes = aligned(i * strip, strip)
        a = jnp.dot(first[...], up[:, lanes], preferred_element_type=F32)
        a = jnp.maximum(a, 0.0)
        activated[:, lanes] = (a * a).astype(BF16)
        return 0

    event(DOWN, 1)
    lax.fori_loop(0, hidden // strip, up_cols, 0)

    def mix_copy(s):
        k = lax.rem(s, per)
        owner = s // per
        return owner, pltpu.make_async_remote_copy(
            src_ref=part.at[s],
            dst_ref=mix.at[me_t, k],
            send_sem=mix_send.at[s],
            recv_sem=mix_recv.at[me_t, k],
            device_id={"tp": owner},
            device_id_type=MESH,
        )

    def down_block(s):
        y = lax.dot_general(
            activated[...],
            down[aligned(s * block, block), :],
            (((1,), (1,)), ((), ())),
            preferred_element_type=F32,
        ).astype(BF16)
        owner, copy = mix_copy(s)

        @pl.when(owner == me_t)
        def _():
            mix[me_t, lax.rem(s, per)] = y

        @pl.when(owner != me_t)
        def _():
            part[s] = y
            copy.start()

    down_block(me)

    def down_step(h, _):
        @pl.when(h > 1)
        def _():
            event(DOWN, 2 * h - 2)
            event(DOWN, 2 * h - 1)

        def side(w, _):
            down_block(at_pos(pos + (2 * w - 1) * h))
            return 0

        lax.fori_loop(0, 2, side, 0)
        return 0

    lax.fori_loop(1, half_n, down_step, 0)
    last_event(DOWN)
    down_block(at_pos(pos + half_n))

    def mix_wait(s, _):
        owner, copy = mix_copy(s)

        @pl.when(owner != me_t)
        def _():
            copy.wait_send()

        return 0

    for d in range(1, t):
        g = lax.rem(me_t + t - d, t)
        for k in range(per):
            dst = mix.at[g, k]
            pltpu.make_async_remote_copy(
                src_ref=dst,
                dst_ref=dst,
                send_sem=mix_send.at[0],
                recv_sem=mix_recv.at[g, k],
                device_id={"tp": peer_t(d)},
                device_id_type=MESH,
            ).wait_recv()

    def second_pre(i, _):
        at = aligned(i * 128, 128)
        sums = jnp.zeros((128, 1), F32)
        squares = jnp.zeros((128, 1), F32)
        x = ALPHA * first[at, aligned(me_t * cols, cols)].astype(F32)
        pieces = []
        for k in range(per):
            v = mix[0, k, at, :].astype(F32)
            for g in range(1, t):
                v = v + mix[g, k, at, :].astype(F32)
            pieces.append(v)
        x = x + (jnp.concatenate(pieces, axis=1) if per > 1 else pieces[0])
        pre[at, pl.ds(0, cols)] = x
        sums = jnp.sum(x, axis=1, keepdims=True)
        squares = jnp.sum(x * x, axis=1, keepdims=True)
        lane = lax.broadcasted_iota(jnp.int32, (128, 128), 1)
        s = jnp.where(lane == 0, sums, jnp.where(lane == 1, squares, 0.0))
        stat[me_t, :, at] = s.T[0:8, :]
        return 0

    for i in range(tok // 128):
        second_pre(i, 0)
    stat_at = lambda g: stat.at[g]
    for d in range(1, t):
        tp_copy(stat.at[me_t], stat_at, stat_send, stat_recv, d).start()

    lax.fori_loop(0, n, mix_wait, 0)
    for item in (KV, UP, DOWN):
        drain_sends(item)

    def br_done(d, _):
        br_copy(d).wait_send()
        return 0

    lax.fori_loop(1, n, br_done, 0)
    for d in range(1, t):
        tp_copy(ow_in, ow_at, ow_send, ow_recv, d).wait_send()
        tp_copy(res_in, res_at, res_send, res_recv, d).wait_send()
        tp_copy(own_att, att_at, att_send, att_recv, d).wait_send()
    for d in range(1, t):
        tp_landed(stat_at, stat_send, stat_recv, d).wait_recv()

    for i in range(tok // 128):
        at = pl.ds(i * 128, 128)
        s = stat[0, :, at]
        for g in range(1, t):
            s = s + stat[g, :, at]
        s = jnp.concatenate([s, jnp.zeros((120, 128), F32)], axis=0).T
        center = s[:, 0:1] / feat
        spread = s[:, 1:2] / feat - center * center
        x = pre[at, pl.ds(0, cols)]
        x = (x - center) * lax.rsqrt(spread + EPSILON)
        out_ref[at, :] = (x * g2_ref[me_t] + b2_ref[me_t]).astype(BF16)
    for d in range(1, t):
        tp_copy(stat.at[me_t], stat_at, stat_send, stat_recv, d).wait_send()


def solution(mesh):
    n, t = mesh.shape["sp"], mesh.shape["tp"]

    def body(
        queries,
        keys,
        values,
        breaks,
        residual_in,
        out_weight,
        first_gain,
        first_shift,
        up_weight,
        down_weight,
        second_gain,
        second_shift,
    ):
        tok, width = queries.shape
        heads = breaks.shape[1]
        feat = out_weight.shape[1]
        cols = residual_in.shape[1]
        hidden = up_weight.shape[1]
        block = up_weight.shape[0]
        per = n // t
        kv = jnp.concatenate([keys, values], axis=1)
        br = jnp.pad(breaks.astype(F32).T, ((0, 8 - heads), (0, 0)))
        any_ = pl.BlockSpec(memory_space=pl.ANY)
        vmem = pl.BlockSpec(memory_space=pltpu.VMEM)
        dma = pltpu.SemaphoreType.DMA
        ring = dma((3, 2, n // 2 + 1, 2))
        return pl.pallas_call(
            functools.partial(layer_kernel, n, t, heads),
            out_shape=jax.ShapeDtypeStruct((tok, cols), BF16),
            in_specs=[vmem, any_, any_, any_, any_, vmem, vmem, any_, any_, vmem, vmem],
            out_specs=vmem,
            scratch_shapes=[
                pltpu.VMEM((n * tok, 2 * width), BF16),
                pltpu.VMEM((feat, hidden), BF16),
                pltpu.VMEM((feat, hidden), BF16),
                pltpu.VMEM((n, 8, tok), F32),
                pltpu.VMEM((t, width, feat), BF16),
                pltpu.VMEM((t, tok, cols), BF16),
                pltpu.VMEM((heads, tok, 128), F32),
                pltpu.VMEM((tok, width), F32),
                pltpu.VMEM((t, tok, width), BF16),
                pltpu.VMEM((tok, tok), BF16),
                pltpu.VMEM((tok, feat), F32),
                pltpu.VMEM((tok, feat), BF16),
                pltpu.VMEM((tok, hidden), BF16),
                pltpu.VMEM((n, tok, block), BF16),
                pltpu.VMEM((t, per, tok, block), BF16),
                pltpu.VMEM((t, 8, tok), F32),
                ring,
                ring,
                dma((n,)),
                dma((n,)),
                dma((t,)),
                dma((t,)),
                dma((t,)),
                dma((t,)),
                dma((t,)),
                dma((t,)),
                dma((n,)),
                dma((t, per)),
                dma((t,)),
                dma((t,)),
                dma((6,)),
            ],
            compiler_params=pltpu.CompilerParams(
                collective_id=0, has_side_effects=True, vmem_limit_bytes=62 * 1024 * 1024
            ),
        )(
            queries,
            kv,
            br,
            residual_in,
            out_weight,
            first_gain.reshape(1, feat),
            first_shift.reshape(1, feat),
            up_weight,
            down_weight,
            second_gain.reshape(t, 1, cols),
            second_shift.reshape(t, 1, cols),
        )

    return jax.shard_map(
        body,
        mesh=mesh,
        in_specs=(
            P("sp", "tp"),
            P("sp", "tp"),
            P("sp", "tp"),
            P("sp", "tp"),
            P("sp", "tp"),
            P("tp", None),
            P(),
            P(),
            P("sp", "tp"),
            P("sp", "tp"),
            P(),
            P(),
        ),
        out_specs=P("sp", "tp"),
        check_vma=False,
    )
```

time: 651 us -> 225 us (0.35)
  waiting for transfers between devices: 423 us -> 0 us
  Pallas kernels: 0 us -> 218 us
  other arithmetic: 99.3 us -> 2.46 us
  matrix products: 49.4 us -> 0 us
  local copies, waits for them, and re-layouts: 36.1 us -> 2.55 us
  blocking collectives: 24.3 us -> 0 us
  between operations: 13.6 us -> 0.01 us
    all_gather x5 -> x0, waiting for transfers between devices: 323 us -> none  [the longest x1 125 us: collect(): lax.all_gather(down_weight, 'sp', axis=0, tiled=True)]
    pallas_call x0 -> x1, Pallas kernels: none -> 218 us  [body(): pl.pallas_call(functools.partial(layer_kernel, n, t, heads), out_shape=ja...]
    psum x1 -> x0, waiting for transfers between devices: 70.5 us -> none  [body(): lax.psum(partial_value.astype(jnp.bfloat16), 'tp').astype(jnp.float32)]
    another operation x21 -> x0, other arithmetic: 70.3 us -> none
    dot_general x16 -> x0, matrix products: 49.4 us -> none  [the longest x7 28.6 us: visit(): jnp.einsum('qhd,khd->hqk', query_heads, key_tile_rows, preferred_element_...]
    reduce_scatter x1 -> x0, waiting for transfers between devices: 28.6 us -> none  [body(): lax.psum_scatter(hidden_partial.astype(jnp.bfloat16), 'tp', scatter_dimen...]
    convert_element_type x10 -> x0, other arithmetic: 21.8 us -> none  [the longest x7 16 us: visit(): jnp.where(strict, jnp.exp(log_break + later), 0.0).astype(jnp.bfloat16)]
    all_gather x1 -> x0, blocking collectives: 18.5 us -> none  [attend(): lax.all_gather(breaks, 'sp', axis=0, tiled=True)]
  transfers between devices with their start and end apart: 7 -> 0, of which waited for: 6 -> 0; matrix products, arithmetic and copies ran while one was open for 23% -> 0% of each run, Pallas kernels for 0% -> 0%
where the time goes in v1:
time: 225 us; the launch traced here: 223 us
  Pallas kernels  218 us (97%)
  local copies, waits for them, and re-layouts  2.55 us (1%)
  other arithmetic  2.46 us (1%)
    pallas_call x1, Pallas kernels, body(): pl.pallas_call(functools.partial(layer_kernel, n, t, heads), out_shape=ja...  218 us

profile of v1, /device:TPU:27, one launch (start us, length us, event | category | flops | bytes accessed | tf_op | source)
XLA Modules:
  0.0 222.5 jit_solution(16320019444450343574)
XLA Ops:
  0.0 0.0 copy-start
  0.0 0.7 copy-done
  0.7 0.6 pad_convert_fusion.br_in
  1.3 1.9 pad_maximum_fusion.kv_in
  3.1 217.5 %shard_map.118 = bf16[512,512]{1,0:T(8,128)(2,1)} custom-call(bf16[512,256]{1,0:T(8,128)(2,1)} %q_ref.1, bf16[512,512]{1,0:T(8,128)(2,1)} %pad_maximum_fusion.kv_in, f32[8,512]{1,0:T(8,128)} %pad_convert_fusion.br_in, bf16[512,512]{1,0:T(8,128)(2,1)} %res_in.1, bf16[256,2048]{1,0:T(8,128)(2,1)} %ow_in.1, f32[1,2048]{1,0:T(1,128)} %bitcast.5, ...), custom_call_target="tpu_custom_call" | custom-call | tf_op jit(solution)/shard_map/pallas_call | solution.py:529
  220.7 1.9 copy.14
Async XLA Ops:
  0.0 0.7 copy-start

commit v2 on v1

v2 whole, which is shorter than its diff:
```python
import functools

import jax
import jax.numpy as jnp
from jax import lax
from jax.experimental import pallas as pl
from jax.experimental.pallas import tpu as pltpu
from jax.sharding import PartitionSpec as P

ALPHA = 2.0**0.25
EPSILON = 1e-05
MESH = pl.DeviceIdType.MESH
F32 = jnp.float32
BF16 = jnp.bfloat16
KV, UP, DOWN = 0, 1, 2


def aligned(start, size):
    return pl.ds(pl.multiple_of(start, size), size)


def layer_kernel(
    n,
    t,
    heads,
    q_ref,
    kv_in,
    br_in,
    res_in,
    ow_in,
    g1_ref,
    b1_ref,
    up_in,
    down_in,
    g2_ref,
    b2_ref,
    out_ref,
    kv,
    up,
    down,
    br,
    ow,
    res,
    later_sum,
    totals,
    att_all,
    lower,
    pre,
    first,
    activated,
    part,
    mix,
    stat,
    up_send,
    up_recv,
    down_send,
    down_recv,
    cross_send,
    cross_recv,
    kvx_send,
    kvx_recv,
    br_send,
    br_recv,
    spread_send,
    spread_recv,
    quarter_send,
    quarter_recv,
    mix_send,
    mix_recv,
    stat_send,
    stat_recv,
    local_sem,
):
    me = lax.axis_index("sp")
    me_t = lax.axis_index("tp")
    tok = q_ref.shape[0]
    width = q_ref.shape[1]
    hd = width // heads
    feat = first.shape[2]
    cols = feat // t
    block = feat // n
    per = n // t
    layers = n // 2
    part_hidden = up.shape[1]
    z, y = me // 2, lax.rem(me, 2)
    partner = 2 * z + 1 - y
    x_count = t // 2
    x, core = me_t // 2, lax.rem(me_t, 2)
    half = tok // 2
    full = (kv, up, down)
    own_in = (kv_in, up_in, down_in)

    def remote(src, dst, send, recv, sp=None, tp=None):
        where = {}
        if sp is not None:
            where["sp"] = sp
        if tp is not None:
            where["tp"] = tp
        return pltpu.make_async_remote_copy(
            src_ref=src,
            dst_ref=dst,
            send_sem=send,
            recv_sem=recv,
            device_id=where,
            device_id_type=MESH,
        )

    def slot(item, layer, piece):
        source = 2 * layer + (y if piece == 0 else 1 - y)
        if item == KV:
            return kv.at[aligned(source * tok + y * half, half)]
        return full[item].at[aligned(source * block, block)]

    def own_piece(item):
        if item == KV:
            return kv_in.at[aligned(y * half, half)]
        return own_in[item].at[:, aligned(y * part_hidden, part_hidden)]

    def climb(item, hop, piece, own=False):
        dst = slot(item, z + 1 - hop, piece)
        return remote(
            own_piece(item) if own else dst,
            dst,
            up_send.at[item, hop, piece],
            up_recv.at[item, hop, piece],
            sp=lax.rem(me + 2, n),
        )

    def climbed(item, hop, piece):
        dst = slot(item, z - hop, piece)
        return remote(
            dst, dst, up_send.at[item, hop, piece], up_recv.at[item, hop, piece], sp=lax.rem(me + 2, n)
        )

    def sink(item, hop, piece, own=False):
        dst = slot(item, z - 1 + hop, piece)
        return remote(
            own_piece(item) if own else dst,
            dst,
            down_send.at[item, hop, piece],
            down_recv.at[item, hop, piece],
            sp=lax.rem(me + n - 2, n),
        )

    def sunk(item, hop, piece):
        dst = slot(item, z + hop, piece)
        return remote(
            dst,
            dst,
            down_send.at[item, hop, piece],
            down_recv.at[item, hop, piece],
            sp=lax.rem(me + n - 2, n),
        )

    def cross(item, landed=False):
        source = partner if landed else me
        dst = full[item].at[aligned(source * block, block)]
        src = own_in[item].at[:, aligned((1 - y) * part_hidden, part_hidden)]
        return remote(dst if landed else src, dst, cross_send.at[item], cross_recv.at[item], sp=partner)

    def cross_kv(which, landed=False):
        source = partner if landed else me
        receiver_y = y if landed else 1 - y
        h = receiver_y if which == 0 else 1 - receiver_y
        dst = kv.at[aligned(source * tok + h * half, half)]
        src = dst if landed else kv_in.at[aligned(h * half, half)]
        return remote(src, dst, kvx_send.at[0, which], kvx_recv.at[0, which], sp=partner)

    def cross_kv_hop(hop, piece, landed=False):
        if landed:
            source = 2 * (z - hop) + (1 - y if piece == 0 else y)
            dst = kv.at[aligned(source * tok + (1 - y) * half, half)]
        else:
            dst = slot(KV, z - hop, piece)
        return remote(dst, dst, kvx_send.at[hop, piece], kvx_recv.at[hop, piece], sp=partner)

    can_up = z + 1 < layers
    can_down = z > 0

    def start_up(item):
        @pl.when(can_up)
        def _():
            climb(item, 1, 0, own=True).start()
            climb(item, 1, 1).start()

    def start_down(item):
        @pl.when(can_down)
        def _():
            sink(item, 1, 0, own=True).start()
            sink(item, 1, 1).start()

    def kv_hop(hop):
        for piece in range(2):

            @pl.when(z - hop >= 0)
            def _():
                climbed(KV, hop, piece).wait_recv()

                @pl.when(can_up)
                def _():
                    climb(KV, hop + 1, piece).start()

                cross_kv_hop(hop, piece).start()

    def event(item, hop, piece):
        @pl.when(z - hop >= 0)
        def _():
            climbed(item, hop, piece).wait_recv()

            @pl.when(can_up)
            def _():
                climb(item, hop + 1, piece).start()

        @pl.when(z + hop < layers)
        def _():
            sunk(item, hop, piece).wait_recv()

            @pl.when(can_down)
            def _():
                sink(item, hop + 1, piece).start()

    def drain_sends(item):
        def one(hop, _):
            for piece in range(2):

                @pl.when(jnp.logical_and(can_up, z + 1 - hop >= 0))
                def _():
                    climb(item, hop, piece).wait_send()

                if item != KV:

                    @pl.when(jnp.logical_and(can_down, z - 1 + hop < layers))
                    def _():
                        sink(item, hop, piece).wait_send()
                else:

                    @pl.when(z - hop >= 0)
                    def _():
                        cross_kv_hop(hop, piece).wait_send()

            return 0

        lax.fori_loop(1, layers, one, 0)

    def spread_copy(kind, at, stage, d, src=None):
        if stage == 0:
            dst = at(me_t)
            to = lax.rem(x + d, x_count) * 2 + core
            i = d
        else:
            dst = at(lax.rem(x + x_count - d, x_count) * 2 + core)
            to = x * 2 + 1 - core
            i = x_count + d
        return remote(
            dst if src is None else src, dst, spread_send.at[kind, i], spread_recv.at[kind, i], tp=to
        )

    def spread_landed(kind, at, stage, d):
        if stage == 0:
            dst = at(lax.rem(x + x_count - d, x_count) * 2 + core)
            to = lax.rem(x + d, x_count) * 2 + core
            i = d
        else:
            dst = at(lax.rem(x + x_count - d, x_count) * 2 + 1 - core)
            to = x * 2 + 1 - core
            i = x_count + d
        return remote(dst, dst, spread_send.at[kind, i], spread_recv.at[kind, i], tp=to)

    def spread_start(kind, at, src=None):
        for d in range(1, x_count):
            spread_copy(kind, at, 0, d, src).start()
        spread_copy(kind, at, 1, 0, src).start()

    def spread_forward(kind, at):
        for d in range(1, x_count):
            spread_landed(kind, at, 0, d).wait_recv()
            spread_copy(kind, at, 1, d).start()

    def spread_finish(kind, at):
        for d in range(x_count):
            spread_landed(kind, at, 1, d).wait_recv()

    def spread_drain(kind, at):
        for d in range(1, x_count):
            spread_copy(kind, at, 0, d).wait_send()
        for d in range(x_count):
            spread_copy(kind, at, 1, d).wait_send()

    OW, RES, ATT, FIRST = range(4)
    ow_at = lambda g: ow.at[g]
    res_at = lambda g: res.at[g]
    att_at = lambda g: att_all.at[g]
    far_at = lambda g: first.at[1 - y, :, aligned(g * cols, cols)]

    def peer_t(d):
        return lax.rem(me_t + d, t)

    def br_copy(d, landed=False):
        owner = lax.rem(me + n - d, n) if landed else me
        return remote(
            br.at[owner] if landed else br_in,
            br.at[owner],
            br_send.at[d],
            br_recv.at[d],
            sp=lax.rem(me + d, n),
        )

    barrier = pltpu.get_barrier_semaphore()

    def greet(d, _):
        pl.semaphore_signal(
            barrier, inc=1, device_id={"sp": lax.rem(me + d, n)}, device_id_type=MESH
        )
        return 0

    lax.fori_loop(1, n, greet, 0)
    for d in range(1, t):
        pl.semaphore_signal(barrier, inc=1, device_id={"tp": peer_t(d)}, device_id_type=MESH)
        pl.semaphore_signal(
            barrier, inc=1, device_id={"sp": partner, "tp": peer_t(d)}, device_id_type=MESH
        )

    own_half = aligned(y * part_hidden, part_hidden)
    locals_ = [
        pltpu.make_async_copy(kv_in, kv.at[aligned(me * tok, tok)], local_sem.at[0]),
        pltpu.make_async_copy(
            up_in.at[:, own_half], up.at[aligned(me * block, block)], local_sem.at[1]
        ),
        pltpu.make_async_copy(
            down_in.at[:, own_half], down.at[aligned(me * block, block)], local_sem.at[2]
        ),
        pltpu.make_async_copy(br_in, br.at[me], local_sem.at[3]),
        pltpu.make_async_copy(res_in, res.at[me_t], local_sem.at[4]),
        pltpu.make_async_copy(ow_in, ow.at[me_t], local_sem.at[5]),
    ]
    pl.semaphore_wait(barrier, n - 1 + 2 * (t - 1))

    @pl.when(can_up)
    def _():
        climb(KV, 1, 0, own=True).start()

    cross_kv(0).start()

    @pl.when(can_down)
    def _():
        sink(UP, 1, 0, own=True).start()

    cross_kv(1).start()
    cross(UP).start()
    cross(DOWN).start()

    def send_breaks(d, _):
        br_copy(d).start()
        return 0

    lax.fori_loop(1, n, send_breaks, 0)
    for c in locals_:
        c.start()
    spread_start(RES, res_at, res_in)
    spread_start(OW, ow_at, ow_in)

    key_row = lax.broadcasted_iota(jnp.int32, (tok, tok), 0)
    key_col = lax.broadcasted_iota(jnp.int32, (tok, tok), 1)
    lower[...] = jnp.where(key_row > key_col, 1.0, 0.0).astype(BF16)
    later_sum[...] = jnp.zeros_like(later_sum)
    totals[...] = jnp.zeros_like(totals)

    cross_kv(0, landed=True).wait_recv()

    @pl.when(can_up)
    def _():
        climb(KV, 1, 1).start()

    cross_kv(1, landed=True).wait_recv()
    cross(UP, landed=True).wait_recv()

    @pl.when(can_down)
    def _():
        sink(UP, 1, 1).start()

    def kv_event(hop, _):
        @pl.when(hop == layers - 1)
        def _():
            start_up(UP)

        kv_hop(hop)
        return 0

    lax.fori_loop(1, layers, kv_event, 0)
    spread_forward(RES, res_at)
    spread_forward(OW, ow_at)

    def kv_rest(hop, _):
        for piece in range(2):

            @pl.when(z - hop >= 0)
            def _():
                cross_kv_hop(hop, piece, landed=True).wait_recv()

        return 0

    lax.fori_loop(1, layers, kv_rest, 0)

    def wait_breaks(d, _):
        br_copy(d, landed=True).wait_recv()
        return 0

    lax.fori_loop(1, n, wait_breaks, 0)
    for c in locals_:
        c.wait()
    cross(DOWN, landed=True).wait_recv()

    scale = hd ** (-0.5)
    tile = 128

    def attend_block(j):
        b = me - j
        for h in range(heads):
            def rows(i, _):
                at = aligned(i * tile, tile)
                keys = kv[aligned(b * tok, tok), pl.ds(h * hd, hd)]
                vals = kv[aligned(b * tok, tok), pl.ds(width + h * hd, hd)]
                z = lax.dot_general(
                    q_ref[at, pl.ds(h * hd, hd)],
                    keys,
                    (((1,), (1,)), ((), ())),
                    preferred_element_type=F32,
                )
                z = z * scale + br[b, pl.ds(h, 1), :]
                soft = jnp.log(1.0 + jnp.exp(-jnp.abs(z)))
                log_break = jnp.minimum(z, 0.0) - soft
                r = lax.broadcasted_iota(jnp.int32, (tile, tok), 0) + i * tile + j * tok
                strict = lax.broadcasted_iota(jnp.int32, (tile, tok), 1) < r
                log_keep = jnp.where(strict, log_break - z, 0.0)
                high = log_keep.astype(BF16)
                low = (log_keep - high.astype(F32)).astype(BF16)
                tri = lower[...]
                later = jnp.dot(high, tri, preferred_element_type=F32) + jnp.dot(
                    low, tri, preferred_element_type=F32
                )
                before = later_sum[h, at, :]
                w = jnp.exp(log_break + later + before[:, 0:1])
                w = jnp.where(strict, w, 0.0).astype(BF16)
                totals[at, pl.ds(h * hd, hd)] += jnp.dot(w, vals, preferred_element_type=F32)
                later_sum[h, at, :] = before + jnp.sum(log_keep, axis=1, keepdims=True)
                return 0

            lax.fori_loop(0, tok // tile, rows, 0)

    def up_event(e):
        hop = 1 + e // 2
        for piece in range(2):

            @pl.when(lax.rem(e, 2) == piece)
            def _():
                event(UP, hop, piece)

        @pl.when(e == 2 * layers - 4)
        def _():
            start_up(DOWN)
            start_down(DOWN)

    def attend_step(j, _):
        @pl.when(j <= me)
        def _():
            attend_block(j)

        @pl.when(j < 2 * layers - 2)
        def _():
            up_event(j)

        return 0

    lax.fori_loop(0, n, attend_step, 0)

    att_all[me_t] = totals[...].astype(BF16)
    spread_start(ATT, att_at)
    spread_finish(OW, ow_at)
    spread_finish(RES, res_at)
    spread_forward(ATT, att_at)
    spread_finish(ATT, att_at)

    big = 256

    def mix_rows(i, _):
        at = aligned(i * big, big)
        for c in range(t):
            lanes = pl.ds(c * cols, cols)
            acc = ALPHA * res[c, at, :].astype(F32)
            mixed = jnp.zeros((big, cols), F32)
            for g in range(t):
                mixed = mixed + jnp.dot(
                    att_all[g, at, :], ow[g, :, lanes], preferred_element_type=F32
                ).astype(BF16).astype(F32)
            pre[at, lanes] = acc + mixed
        return 0

    lax.fori_loop(0, tok // big, mix_rows, 0)

    small = 64

    def norm_rows(i, _):
        at = aligned(i * small, small)
        v = pre[at, :]
        center = jnp.sum(v, axis=1, keepdims=True) / feat
        v = v - center
        spread = jnp.sum(v * v, axis=1, keepdims=True) / feat
        first[y, at, :] = (v * lax.rsqrt(spread + EPSILON) * g1_ref[...] + b1_ref[...]).astype(BF16)
        return 0

    lax.fori_loop(0, tok // small, norm_rows, 0)

    def quarter(landed=False):
        dst = first.at[1 - y if landed else y, :, aligned(me_t * cols, cols)]
        return remote(dst, dst, quarter_send.at[0], quarter_recv.at[0], sp=partner)

    quarter().start()
    event(DOWN, 1, 0)

    strip = 256

    def up_side(a):
        def up_cols(i, _):
            lanes = aligned(i * strip, strip)
            v = jnp.dot(first[a], up[:, lanes], preferred_element_type=F32)
            v = jnp.maximum(v, 0.0)
            activated[a, :, lanes] = (v * v).astype(BF16)
            return 0

        lax.fori_loop(0, part_hidden // strip, up_cols, 0)

    up_side(y)
    quarter(landed=True).wait_recv()
    spread_start(FIRST, far_at)
    event(DOWN, 1, 1)
    spread_forward(FIRST, far_at)
    spread_finish(FIRST, far_at)
    up_side(1 - y)

    def mix_copy(s, a):
        k = lax.rem(s, per)
        owner = s // per
        return owner, remote(
            part.at[s, a],
            mix.at[y * t + me_t, k],
            mix_send.at[s, a],
            mix_recv.at[y * t + me_t, k],
            sp=2 * z + a,
            tp=owner,
        )

    def down_block(s):
        def side(i, _):
            a = lax.rem(y + 1 + i, 2)
            v = lax.dot_general(
                activated[a],
                down[aligned(s * block, block), :],
                (((1,), (1,)), ((), ())),
                preferred_element_type=F32,
            ).astype(BF16)
            owner, copy = mix_copy(s, a)
            mine = jnp.logical_and(owner == me_t, a == y)

            @pl.when(mine)
            def _():
                mix[y * t + me_t, lax.rem(s, per)] = v

            @pl.when(jnp.logical_not(mine))
            def _():
                part[s, a] = v
                copy.start()

            return 0

        lax.fori_loop(0, 2, side, 0)

    down_block(me)
    down_block(partner)

    def down_step(hop, _):
        for piece in range(2):

            @pl.when(hop > 1)
            def _():
                event(DOWN, hop, piece)

            c = y if piece == 0 else 1 - y

            @pl.when(z - hop >= 0)
            def _():
                down_block(2 * (z - hop) + c)

            @pl.when(z + hop < layers)
            def _():
                down_block(2 * (z + hop) + c)

        return 0

    lax.fori_loop(1, layers, down_step, 0)

    def mix_wait(s, _):
        for a in range(2):
            owner, copy = mix_copy(s, a)

            @pl.when(jnp.logical_not(jnp.logical_and(owner == me_t, a == y)))
            def _():
                copy.wait_send()

        return 0

    def mix_landed(g, k):
        dst = mix.at[g, k]
        remote(dst, dst, mix_send.at[0, 0], mix_recv.at[g, k], sp=partner).wait_recv()

    for k in range(per):
        for d in range(1, t):
            mix_landed(y * t + lax.rem(me_t + t - d, t), k)
        for d in range(t):
            mix_landed((1 - y) * t + lax.rem(me_t + t - d, t), k)

    for i in range(tok // 128):
        at = pl.ds(i * 128, 128)
        v = ALPHA * first[y, at, aligned(me_t * cols, cols)].astype(F32)
        pieces = []
        for k in range(per):
            u = mix[0, k, at, :].astype(F32)
            for g in range(1, 2 * t):
                u = u + mix[g, k, at, :].astype(F32)
            pieces.append(u)
        v = v + (jnp.concatenate(pieces, axis=1) if per > 1 else pieces[0])
        pre[at, pl.ds(0, cols)] = v
        sums = jnp.sum(v, axis=1, keepdims=True)
        squares = jnp.sum(v * v, axis=1, keepdims=True)
        lane = lax.broadcasted_iota(jnp.int32, (128, 128), 1)
        both = jnp.where(lane == 0, sums, jnp.where(lane == 1, squares, 0.0))
        stat[me_t, :, at] = both.T[0:8, :]

    def stat_copy(d, landed=False):
        dst = stat.at[lax.rem(me_t + t - d, t) if landed else me_t]
        return remote(dst, dst, stat_send.at[d], stat_recv.at[d], tp=peer_t(d))

    for d in range(1, t):
        stat_copy(d).start()

    lax.fori_loop(0, n, mix_wait, 0)
    for item in (KV, UP, DOWN):
        drain_sends(item)
    cross_kv(0).wait_send()
    cross_kv(1).wait_send()
    cross(UP).wait_send()
    cross(DOWN).wait_send()
    quarter().wait_send()

    def br_done(d, _):
        br_copy(d).wait_send()
        return 0

    lax.fori_loop(1, n, br_done, 0)
    spread_drain(OW, ow_at)
    spread_drain(RES, res_at)
    spread_drain(ATT, att_at)
    spread_drain(FIRST, far_at)
    for d in range(1, t):
        stat_copy(d, landed=True).wait_recv()

    for i in range(tok // 128):
        at = pl.ds(i * 128, 128)
        v = stat[0, :, at]
        for g in range(1, t):
            v = v + stat[g, :, at]
        v = jnp.concatenate([v, jnp.zeros((120, 128), F32)], axis=0).T
        center = v[:, 0:1] / feat
        spread = v[:, 1:2] / feat - center * center
        u = (pre[at, pl.ds(0, cols)] - center) * lax.rsqrt(spread + EPSILON)
        out_ref[at, :] = (u * g2_ref[me_t] + b2_ref[me_t]).astype(BF16)
    for d in range(1, t):
        stat_copy(d).wait_send()


def solution(mesh):
    n, t = mesh.shape["sp"], mesh.shape["tp"]

    def body(
        queries,
        keys,
        values,
        breaks,
        residual_in,
        out_weight,
        first_gain,
        first_shift,
        up_weight,
        down_weight,
        second_gain,
        second_shift,
    ):
        tok, width = queries.shape
        heads = breaks.shape[1]
        feat = out_weight.shape[1]
        cols = residual_in.shape[1]
        hidden = up_weight.shape[1]
        block = up_weight.shape[0]
        per = n // t
        kv = jnp.concatenate([keys, values], axis=1)
        br = jnp.pad(breaks.astype(F32).T, ((0, 8 - heads), (0, 0)))
        any_ = pl.BlockSpec(memory_space=pl.ANY)
        vmem = pl.BlockSpec(memory_space=pltpu.VMEM)
        dma = pltpu.SemaphoreType.DMA
        ring = dma((3, n // 2 + 1, 2))
        return pl.pallas_call(
            functools.partial(layer_kernel, n, t, heads),
            out_shape=jax.ShapeDtypeStruct((tok, cols), BF16),
            in_specs=[vmem, any_, any_, any_, any_, vmem, vmem, any_, any_, vmem, vmem],
            out_specs=vmem,
            scratch_shapes=[
                pltpu.VMEM((n * tok, 2 * width), BF16),
                pltpu.VMEM((feat, hidden // 2), BF16),
                pltpu.VMEM((feat, hidden // 2), BF16),
                pltpu.VMEM((n, 8, tok), F32),
                pltpu.VMEM((t, width, feat), BF16),
                pltpu.VMEM((t, tok, cols), BF16),
                pltpu.VMEM((heads, tok, 128), F32),
                pltpu.VMEM((tok, width), F32),
                pltpu.VMEM((t, tok, width), BF16),
                pltpu.VMEM((tok, tok), BF16),
                pltpu.VMEM((tok, feat), F32),
                pltpu.VMEM((2, tok, feat), BF16),
                pltpu.VMEM((2, tok, hidden // 2), BF16),
                pltpu.VMEM((n, 2, tok, block), BF16),
                pltpu.VMEM((2 * t, per, tok, block), BF16),
                pltpu.VMEM((t, 8, tok), F32),
                ring,
                ring,
                ring,
                ring,
                dma((3,)),
                dma((3,)),
                dma((n // 2, 2)),
                dma((n // 2, 2)),
                dma((n,)),
                dma((n,)),
                dma((4, t)),
                dma((4, t)),
                dma((1,)),
                dma((1,)),
                dma((n, 2)),
                dma((2 * t, per)),
                dma((t,)),
                dma((t,)),
                dma((6,)),
            ],
            compiler_params=pltpu.CompilerParams(
                collective_id=0, has_side_effects=True, vmem_limit_bytes=62 * 1024 * 1024
            ),
        )(
            queries,
            kv,
            br,
            residual_in,
            out_weight,
            first_gain.reshape(1, feat),
            first_shift.reshape(1, feat),
            up_weight,
            down_weight,
            second_gain.reshape(t, 1, cols),
            second_shift.reshape(t, 1, cols),
        )

    return jax.shard_map(
        body,
        mesh=mesh,
        in_specs=(
            P("sp", "tp"),
            P("sp", "tp"),
            P("sp", "tp"),
            P("sp", "tp"),
            P("sp", "tp"),
            P("tp", None),
            P(),
            P(),
            P("sp", "tp"),
            P("sp", "tp"),
            P(),
            P(),
        ),
        out_specs=P("sp", "tp"),
        check_vma=False,
    )
```

time: 225 us -> 239 us (1.062); the launches traced: 223 us -> 239 us
  Pallas kernels: 218 us -> 234 us
    pallas_call x1, Pallas kernels: 218 us -> 234 us  [body(): pl.pallas_call(functools.partial(layer_kernel, n, t, heads), out_shape=ja...]
where the time goes in v2:
time: 239 us
  Pallas kernels  234 us (98%)
  local copies, waits for them, and re-layouts  2.55 us (1%)
  other arithmetic  2.46 us (1%)
    pallas_call x1, Pallas kernels, body(): pl.pallas_call(functools.partial(layer_kernel, n, t, heads), out_shape=ja...  234 us

profile of v2, /device:TPU:27, one launch (start us, length us, event | category | flops | bytes accessed | tf_op | source)
XLA Modules:
  0.0 239.0 jit_solution(2266747350809847401)
XLA Ops:
  0.0 0.0 copy-start
  0.0 0.7 copy-done
  0.7 0.6 pad_convert_fusion.br_in
  1.3 1.9 pad_maximum_fusion.kv_in
  3.1 234.0 %shard_map.118 = bf16[512,512]{1,0:T(8,128)(2,1)} custom-call(bf16[512,256]{1,0:T(8,128)(2,1)} %q_ref.1, bf16[512,512]{1,0:T(8,128)(2,1)} %pad_maximum_fusion.kv_in, f32[8,512]{1,0:T(8,128)} %pad_convert_fusion.br_in, bf16[512,512]{1,0:T(8,128)(2,1)} %res_in.1, bf16[256,2048]{1,0:T(8,128)(2,1)} %ow_in.1, f32[1,2048]{1,0:T(1,128)} %bitcast.5, ...), custom_call_target="tpu_custom_call" | custom-call | tf_op jit(solution)/shard_map/pallas_call | solution.py:710
  237.2 1.9 copy.14
Async XLA Ops:
  0.0 0.7 copy-start

commit v3 on v2

--- a/solution.py
+++ b/solution.py
@@ -451,11 +451,11 @@
         hop = 1 + e // 2
         for piece in range(2):
 
-            @pl.when(lax.rem(e, 2) == piece)
+            @pl.when(lax.rem(jnp.int32(e), 2) == piece)
             def _():
                 event(UP, hop, piece)
 
-        @pl.when(e == 2 * layers - 4)
+        @pl.when(jnp.int32(e) == 2 * layers - 4)
         def _():
             start_up(DOWN)
             start_down(DOWN)
@@ -465,7 +465,7 @@
         def _():
             attend_block(j)
 
-        @pl.when(j < 2 * layers - 2)
+        @pl.when(j < 2 * layers - 5)
         def _():
             up_event(j)
 
@@ -475,6 +475,7 @@
 
     att_all[me_t] = totals[...].astype(BF16)
     spread_start(ATT, att_at)
+    up_event(2 * layers - 5)
     spread_finish(OW, ow_at)
     spread_finish(RES, res_at)
     spread_forward(ATT, att_at)
@@ -496,6 +497,7 @@
         return 0
 
     lax.fori_loop(0, tok // big, mix_rows, 0)
+    up_event(2 * layers - 4)
 
     small = 64
 
@@ -515,6 +517,7 @@
         return remote(dst, dst, quarter_send.at[0], quarter_recv.at[0], sp=partner)
 
     quarter().start()
+    up_event(2 * layers - 3)
     event(DOWN, 1, 0)
 
     strip = 256

time: 239 us -> 228 us (0.954)
  Pallas kernels: 234 us -> 222 us
    pallas_call x1, Pallas kernels: 234 us -> 222 us  [body(): pl.pallas_call(functools.partial(layer_kernel, n, t, heads), out_shape=ja...]
where the time goes in v3:
time: 228 us; the launch traced here: 227 us
  Pallas kernels  222 us (97%)
  local copies, waits for them, and re-layouts  2.55 us (1%)
  other arithmetic  2.46 us (1%)
    pallas_call x1, Pallas kernels, body(): pl.pallas_call(functools.partial(layer_kernel, n, t, heads), out_shape=ja...  222 us

profile of v3, /device:TPU:27, one launch (start us, length us, event | category | flops | bytes accessed | tf_op | source)
XLA Modules:
  0.0 227.4 jit_solution(4303305518274273957)
XLA Ops:
  0.0 0.0 copy-start
  0.0 0.7 copy-done
  0.7 0.6 pad_convert_fusion.br_in
  1.3 1.9 pad_maximum_fusion.kv_in
  3.1 222.4 %shard_map.118 = bf16[512,512]{1,0:T(8,128)(2,1)} custom-call(bf16[512,256]{1,0:T(8,128)(2,1)} %q_ref.1, bf16[512,512]{1,0:T(8,128)(2,1)} %pad_maximum_fusion.kv_in, f32[8,512]{1,0:T(8,128)} %pad_convert_fusion.br_in, bf16[512,512]{1,0:T(8,128)(2,1)} %res_in.1, bf16[256,2048]{1,0:T(8,128)(2,1)} %ow_in.1, f32[1,2048]{1,0:T(1,128)} %bitcast.5, ...), custom_call_target="tpu_custom_call" | custom-call | tf_op jit(solution)/shard_map/pallas_call | solution.py:713
  225.5 1.9 copy.14
Async XLA Ops:
  0.0 0.7 copy-start
